TPU v7x, 512 devices: a whole 4x4x16 slice. The times are simulated.
512 devices in a mesh: ep: 128 (over z, x, core), tp: 4 (over y).
Axes of the slice: x: 4, y: 4, z: 16, core: 2. Of those that a mesh axis runs over, the one named last changes fastest.
Arguments:
- tokens: bfloat16 [2048, 1024], P('ep'), may hold values from -6 to 6
- old_state: float32 [2048, 4, 128, 128], P('ep', 'tp'), may hold values from -6 to 6
- query_weight: bfloat16 [1024, 512], P(None, 'tp'), may hold values from -0.1875 to 0.1875
- forget_weight: bfloat16 [1024, 512], P(None, 'tp'), may hold values from -0.1875 to 0.1875
- input_weight: bfloat16 [1024, 512], P(None, 'tp'), may hold values from -0.1875 to 0.1875
- lower_bound: float32 [512], P('tp'), may hold values from 0 to 0.9
- head_gain: float32 [4, 128], P('tp'), may hold values from 0.1 to 1.9
- out_weight: bfloat16 [512, 1024], P('tp'), may hold values from -0.25 to 0.25
- mix_gain: float32 [1024], replicated, may hold values from 0.1 to 1.9
- ffn_gain: float32 [1024], replicated, may hold values from 0.1 to 1.9
- group_weight: bfloat16 [1024, 4], replicated, may hold values from -0.1875 to 0.1875
- expert_weight: bfloat16 [1024, 128], replicated, may hold values from -0.1875 to 0.1875
- routes: int32 [2048, 6], P('ep'), may hold values from 0 to 127, all different within a row; in each aligned block of 16 rows (0 to 15, 16 to 31, ...) at most 2 rows name the same one
- gate_weight: bfloat16 [128, 1024, 1024], P('ep', None, 'tp'), may hold values from -0.1875 to 0.1875
- up_weight: bfloat16 [128, 1024, 1024], P('ep', None, 'tp'), may hold values from -0.1875 to 0.1875
- down_weight: bfloat16 [128, 1024, 1024], P('ep', None, 'tp'), may hold values from -0.1875 to 0.1875
Outputs:
- layer_out: bfloat16 [2048, 1024], P('ep', 'tp')
- new_state: float32 [2048, 4, 128, 128], P('ep', 'tp')
Inputs may be any that keep to these rules, and one draw needn't show every extreme that they name: `routes`: each row names 6 different experts. In each aligned block of 16 rows (the rows of one device) no expert is named more than 2 times, a bound that some block reaches.
All inputs are finite; a program needn't handle non-finite values.
Results may differ from a plain program's by a relative error of at most 0.011.
Values may be sent and summed in bfloat16 or wider, within the bound.
A program may use at most 64 MiB of HBM per device.

v0:
```python
import jax
import jax.numpy as jnp
from jax import lax
from jax.sharding import PartitionSpec as P

epsilon = 1e-06


def from_everyone(array, axis):
    count = lax.axis_size(axis)
    return lax.all_to_all(
        jnp.broadcast_to(array[None], (count, *array.shape)), axis, 0, 0, tiled=True
    )


def over_copies(array, axis):
    return from_everyone(array, axis).astype(jnp.float32).sum(axis=0)


def laid_out(blocks, dim):
    blocks = jnp.moveaxis(blocks, 0, dim)
    lengths = blocks.shape
    return blocks.reshape(*lengths[:dim], lengths[dim] * lengths[dim + 1], *lengths[dim + 2 :])


def gathered_copies(array, axis, dim):
    return laid_out(from_everyone(array, axis), dim)


def scaled_rms(values, gain):
    return values * lax.rsqrt(jnp.mean(values * values, axis=-1, keepdims=True) + epsilon) * gain


def local(
    tokens,
    old_state,
    query_weight,
    forget_weight,
    input_weight,
    lower_bound,
    head_gain,
    out_weight,
    mix_gain,
    ffn_gain,
    group_weight,
    expert_weight,
    routes,
    gate_weight,
    up_weight,
    down_weight,
):
    seq_count, model_width = tokens.shape
    heads_local, head_size = (old_state.shape[1], old_state.shape[2])
    tp_size = lax.axis_size("tp")
    tp_rank = lax.axis_index("tp")
    part_width = model_width // tp_size
    resident = tokens.astype(jnp.float32)
    normed = scaled_rms(resident, mix_gain).astype(jnp.bfloat16)
    query_pre = jnp.dot(normed, query_weight, preferred_element_type=jnp.float32)
    forget_pre = jnp.dot(normed, forget_weight, preferred_element_type=jnp.float32)
    input_pre = jnp.dot(normed, input_weight, preferred_element_type=jnp.float32)
    query = jax.nn.silu(query_pre).reshape(seq_count, heads_local, head_size)
    forget = (lower_bound + (1.0 - lower_bound) * jax.nn.sigmoid(forget_pre)).reshape(
        seq_count, heads_local, head_size
    )
    value = input_pre.reshape(seq_count, heads_local, head_size)
    new_state = forget[..., None] * old_state + (1.0 - forget)[..., None] * value[:, :, None, :]
    readout = jnp.sum(new_state * query[..., None], axis=2)
    head_out = (
        scaled_rms(readout, head_gain)
        .astype(jnp.bfloat16)
        .reshape(seq_count, heads_local * head_size)
    )
    head_part = jnp.dot(head_out, out_weight, preferred_element_type=jnp.float32)
    mixed = (
        over_copies(head_part.astype(jnp.bfloat16), "tp").astype(jnp.float32).astype(jnp.bfloat16)
    )
    residual = (resident + mixed.astype(jnp.float32)).astype(jnp.bfloat16)
    ffn_in = scaled_rms(residual.astype(jnp.float32), ffn_gain).astype(jnp.bfloat16)
    experts = expert_weight.shape[1]
    groups = group_weight.shape[1]
    top_count = routes.shape[1]
    group_raw = jnp.exp(jnp.dot(ffn_in, group_weight, preferred_element_type=jnp.float32))
    group_prob = group_raw / jnp.sum(group_raw, axis=-1, keepdims=True)
    expert_raw = jnp.exp(
        jnp.dot(ffn_in, expert_weight, preferred_element_type=jnp.float32)
    ).reshape(seq_count, groups, experts // groups)
    expert_prob = (
        expert_raw / jnp.sum(expert_raw, axis=-1, keepdims=True) * group_prob[:, :, None]
    ).reshape(seq_count, experts)
    expert_ids = jnp.arange(experts, dtype=jnp.int32)
    chosen = routes[:, :, None] == expert_ids[None, None, :]
    weight = jnp.sum(jnp.where(chosen, expert_prob[:, None, :], 0.0), axis=-1)
    gate = weight / jnp.sum(weight, axis=-1, keepdims=True)
    capacity = min(seq_count, max(2, 2 * seq_count * top_count // experts))
    flat = routes.reshape(-1)
    hits = (flat[:, None] == expert_ids[None, :]).astype(jnp.int32)
    before = jnp.cumsum(hits, axis=0) - hits
    slots = jnp.sum(hits * before, axis=1)
    target = flat * capacity + slots
    slot_ids = jnp.arange(experts * capacity, dtype=jnp.int32)
    spread = jnp.sum(
        (slot_ids[:, None, None] == target.reshape(seq_count, top_count)[None, :, :]).astype(
            jnp.int32
        ),
        axis=2,
    ).astype(jnp.bfloat16)
    choose = (target[:, None] == slot_ids[None, :]).astype(jnp.bfloat16)
    own_part = lax.dynamic_slice_in_dim(ffn_in, tp_rank * part_width, part_width, 1)
    outgoing = (
        jnp.dot(spread, own_part, preferred_element_type=jnp.float32)
        .astype(jnp.bfloat16)
        .reshape(experts, capacity, part_width)
    )
    partial_rows = lax.all_to_all(outgoing, "ep", split_axis=0, concat_axis=1, tiled=True)
    arrived = gathered_copies(partial_rows, "tp", 2)
    gate_hidden = jnp.einsum(
        "erd,edf->erf", arrived, gate_weight, preferred_element_type=jnp.float32
    )
    up_hidden = jnp.einsum("erd,edf->erf", arrived, up_weight, preferred_element_type=jnp.float32)
    hidden = (jax.nn.silu(gate_hidden) * up_hidden).astype(jnp.bfloat16)
    produced = jnp.einsum(
        "erf,efd->erd",
        gathered_copies(hidden, "tp", 2),
        down_weight,
        preferred_element_type=jnp.float32,
    ).astype(jnp.bfloat16)
    returned = lax.all_to_all(produced, "ep", split_axis=1, concat_axis=0, tiled=True)
    picked = jnp.dot(
        choose, returned.reshape(experts * capacity, part_width), preferred_element_type=jnp.float32
    ).reshape(seq_count, top_count, part_width)
    mixture = jnp.sum(gate[:, :, None] * picked, axis=1)
    own_resid = lax.dynamic_slice_in_dim(residual, tp_rank * part_width, part_width, 1).astype(
        jnp.float32
    )
    layer_out = (own_resid + mixture).astype(jnp.bfloat16)
    return (layer_out, new_state)


def solution(mesh):
    in_specs = (
        P("ep", None),
        P("ep", "tp", None, None),
        P(None, "tp"),
        P(None, "tp"),
        P(None, "tp"),
        P("tp"),
        P("tp", None),
        P("tp", None),
        P(),
        P(),
        P(),
        P(),
        P("ep", None),
        P("ep", None, "tp"),
        P("ep", None, "tp"),
        P("ep", None, "tp"),
    )
    out_specs = (P("ep", "tp"), P("ep", "tp", None, None))
    return jax.shard_map(local, mesh=mesh, in_specs=in_specs, out_specs=out_specs, check_vma=False)
```

profile of v0, /device:TPU:1, one launch (start us, length us, event | category | flops | bytes accessed | tf_op | source)
XLA Modules:
  0.0 113.7 jit_solution(16716922111124903462)
XLA Ops:
  0.6 0.0 copy-start
  0.7 0.9 fusion.20
  1.6 0.7 broadcast_subtract_fusion.1
  2.3 1.2 %divide_multiply_fusion.1 = f32[16,128]{1,0:T(8,128)S(1)} fusion(bf16[1024,128]{1,0:T(8,128)(2,1)} %param.18, bf16[16,1024]{1,0:T(8,128)(2,1)S(1)} %copy-done.1, f32[1024]{0:T(1024)S(1)} %copy-done.6, f32[16]{0:T(128)S(1)} %add_rsqrt_fusion.2), kind=kOutput, calls=%fused_computation.54 | convolution fusion | flops 4268032 | bytes 307264 | tf_op jit(solution)/shard_map/dot_general | solution.py:59
  3.5 0.0 copy-start.8
  3.5 0.2 fusion.33
  3.7 0.0 copy-done.2
  3.7 0.4 copy-done.8
  4.2 0.2 broadcast_subtract_fusion
  4.4 0.0 copy-start.3
  4.4 2.8 %multiply_reduce_fusion = (f32[16,128]{1,0:T(8,128)S(1)}, f32[16,1,128,128]{3,2,1,0:T(8,128)}) fusion(f32[16,128]{1,0:T(8,128)S(1)} %divide_multiply_fusion.1, f32[16,128]{1,0:T(8,128)S(1)} %fusion.33, f32[16,128]{1,0:T(8,128)S(1)} %get-tuple-element.8, f32[16,1,128,128]{3,2,1,0:T(8,128)} %param.17, f32[16,128]{1,0:T(8,128)S(1)} %get-tuple-element.9), kind=kLoop, calls=%fused_computation.17 | loop fusion | flops 1308672 | bytes 2138112 | tf_op jit(solution)/shard_map/reduce_sum | solution.py:68
  7.3 0.1 multiply_reduce_fusion.1
  7.4 0.6 copy-done.9
  8.1 0.2 convolution_convert_fusion.2
  8.2 0.7 broadcast_in_dim.16
  8.9 5.0 %all-to-all-start = ((bf16[4,16,1024]{2,1,0:T(8,128)(2,1)}), bf16[4,16,1024]{2,1,0:T(8,128)(2,1)S(1)}, u32[]{:S(2)}, u32[]{:S(2)}) async-start(bf16[4,16,1024]{2,1,0:T(8,128)(2,1)} %broadcast_in_dim.16), calls=%async_computation | async-start | bytes 262144 | tf_op jit(solution)/shard_map/all_to_all | solution.py:11
  13.9 0.7 copy-done.5
  14.6 0.1 copy.61
  14.7 0.1 eq.73
  14.8 0.1 fusion.25
  14.9 0.1 reduce_window_sum.11
  15.0 0.2 select_reduce_fusion.2
  15.2 0.1 reduce_sum.123
  15.3 0.1 copy.62
  15.4 0.1 convert_reduce_fusion
  15.5 3.3 %all-to-all-done = bf16[4,16,1024]{2,1,0:T(8,128)(2,1)S(1)} async-done(((bf16[4,16,1024]{2,1,0:T(8,128)(2,1)}), bf16[4,16,1024]{2,1,0:T(8,128)(2,1)S(1)}, u32[]{:S(2)}, u32[]{:S(2)}) %all-to-all-start) | async-done | bytes 131104 | tf_op jit(solution)/shard_map/all_to_all | solution.py:11
  18.8 0.1 fusion.17
  18.9 0.7 copy-done.7
  19.6 0.1 fusion.19
  19.7 0.2 convolution_convert_fusion.1
  19.9 0.1 reshape.215
  19.9 37.1 %all_to_all.33 = bf16[128,2,256]{2,1,0:T(2,128)(2,1)S(1)} all-to-all(bf16[128,2,256]{2,1,0:T(2,128)(2,1)S(1)} %reshape.215), channel_id=1, replica_groups=mesh['ep'=128,'tp'=4] {'ep'}, dimensions={0} | all-to-all | bytes 262144 | tf_op jit(solution)/shard_map/all_to_all | solution.py:115
  57.1 0.1 broadcast_in_dim.19
  57.1 0.1 copy.63
  57.2 0.8 broadcast_in_dim.20
  58.1 3.6 %all-to-all-start.2 = ((bf16[4,1,256,256]{2,3,1,0:T(8,128)(2,1)}), bf16[4,1,256,256]{2,3,1,0:T(8,128)(2,1)S(1)}, u32[]{:S(2)}, u32[]{:S(2)}) async-start(bf16[4,1,256,256]{2,3,1,0:T(8,128)(2,1)} %broadcast_in_dim.20), calls=%async_computation.2 | async-start | bytes 1048576 | tf_op jit(solution)/shard_map/all_to_all | solution.py:11
  61.7 0.0 copy-done.13
  61.7 0.1 fusion.39
  61.8 0.1 copy.60
  61.9 0.1 mul.194
  62.0 0.1 mul.195
  62.1 8.7 %all-to-all-done.2 = bf16[4,1,256,256]{2,3,1,0:T(8,128)(2,1)S(1)} async-done(((bf16[4,1,256,256]{2,3,1,0:T(8,128)(2,1)}), bf16[4,1,256,256]{2,3,1,0:T(8,128)(2,1)S(1)}, u32[]{:S(2)}, u32[]{:S(2)}) %all-to-all-start.2) | async-done | bytes 524320 | tf_op jit(solution)/shard_map/all_to_all | solution.py:11
  70.8 0.3 fusion.11
  71.2 0.7 copy-done.10
  71.9 0.3 fusion.1
  72.2 0.1 copy.65
  72.3 0.8 broadcast_in_dim.21
  73.2 3.6 %all-to-all-start.3 = ((bf16[4,1,256,256]{2,3,1,0:T(8,128)(2,1)}), bf16[4,1,256,256]{2,3,1,0:T(8,128)(2,1)S(1)}, u32[]{:S(2)}, u32[]{:S(2)}) async-start(bf16[4,1,256,256]{2,3,1,0:T(8,128)(2,1)} %broadcast_in_dim.21), calls=%async_computation.3 | async-start | bytes 1048576 | tf_op jit(solution)/shard_map/all_to_all | solution.py:11
  76.8 0.2 convolution_exponential_fusion
  76.9 0.1 reshape.214
  77.0 0.1 fusion
  77.1 0.1 div.59
  77.2 7.6 %all-to-all-done.3 = bf16[4,1,256,256]{2,3,1,0:T(8,128)(2,1)S(1)} async-done(((bf16[4,1,256,256]{2,3,1,0:T(8,128)(2,1)}), bf16[4,1,256,256]{2,3,1,0:T(8,128)(2,1)S(1)}, u32[]{:S(2)}, u32[]{:S(2)}) %all-to-all-start.3) | async-done | bytes 524320 | tf_op jit(solution)/shard_map/all_to_all | solution.py:11
  84.8 0.3 fusion.2
  85.1 0.2 copy.74
  85.3 0.5 broadcast.158
  85.8 1.4 %reduce.5 = bf16[256,256]{1,0:T(8,128)(2,1)S(1)} reduce(bf16[256,1,256]{2,1,0:T(2,128)(2,1)S(1)} %bitcast.46, bf16[]{:T(256)} %broadcast.158), dimensions={1}, to_apply=%bitcast.43.reduce_sub_computation | reduce | bytes 262146
  87.3 0.7 reshape.224
  88.0 8.8 %all-to-all-start.4 = ((bf16[128,2,256]{2,1,0:T(2,128)(2,1)}), bf16[128,2,256]{2,1,0:T(2,128)(2,1)S(1)}, u32[]{:S(2)}, u32[]{:S(2)}) async-start(bf16[128,2,256]{2,1,0:T(2,128)(2,1)} %reshape.224), calls=%async_computation.4 | async-start | bytes 262144 | tf_op jit(solution)/shard_map/all_to_all | solution.py:128
  96.8 0.2 select_reduce_fusion
  97.0 15.8 %all-to-all-done.4 = bf16[128,2,256]{2,1,0:T(2,128)(2,1)S(1)} async-done(((bf16[128,2,256]{2,1,0:T(2,128)(2,1)}), bf16[128,2,256]{2,1,0:T(2,128)(2,1)S(1)}, u32[]{:S(2)}, u32[]{:S(2)}) %all-to-all-start.4) | async-done | bytes 131104 | tf_op jit(solution)/shard_map/all_to_all | solution.py:128
  112.8 0.1 reshape.225
  112.9 0.2 fusion.3
  113.1 0.6 add_convert_fusion
  (26 shorter events, 0.1 us)
Async XLA Ops:
  0.6 70.2 %copy-start = (bf16[1,1024,256]{2,1,0:T(8,128)(2,1)S(1)}, bf16[1,1024,256]{2,1,0:T(8,128)(2,1)}, u32[]{:S(2)}) copy-start(bf16[1,1024,256]{2,1,0:T(8,128)(2,1)} %param.29) | copy-start | bytes 1572868
  0.6 1.7 %copy-start.1 = (bf16[16,1024]{1,0:T(8,128)(2,1)S(1)}, bf16[16,1024]{1,0:T(8,128)(2,1)}, u32[]{:S(2)}) copy-start(bf16[16,1024]{1,0:T(8,128)(2,1)} %param.16) | copy-start | bytes 98308
  0.7 1.6 %copy-start.6 = (f32[1024]{0:T(1024)S(1)}, f32[1024]{0:T(1024)}, u32[]{:S(2)}) copy-start(f32[1024]{0:T(1024)} %param.24) | copy-start | bytes 12292
  0.7 2.9 %copy-start.12 = (bf16[1024,128]{1,0:T(8,128)(2,1)S(1)}, bf16[1024,128]{1,0:T(8,128)(2,1)}, u32[]{:S(2)}) copy-start(bf16[1024,128]{1,0:T(8,128)(2,1)} %param.20) | copy-start | bytes 786436
  2.3 1.4 %copy-start.2 = (bf16[1024,128]{1,0:T(8,128)(2,1)S(1)}, bf16[1024,128]{1,0:T(8,128)(2,1)}, u32[]{:S(2)}) copy-start(bf16[1024,128]{1,0:T(8,128)(2,1)} %param.19) | copy-start | bytes 786436
  3.5 0.7 copy-start.8
  4.4 3.0 %copy-start.3 = (bf16[128,1024]{1,0:T(8,128)(2,1)S(1)}, bf16[128,1024]{1,0:T(8,128)(2,1)}, u32[]{:S(2)}) copy-start(bf16[128,1024]{1,0:T(8,128)(2,1)} %param.23) | copy-start | bytes 786436
  7.4 0.7 copy-start.9
  8.9 9.8 %all-to-all-start = ((bf16[4,16,1024]{2,1,0:T(8,128)(2,1)}), bf16[4,16,1024]{2,1,0:T(8,128)(2,1)S(1)}, u32[]{:S(2)}, u32[]{:S(2)}) async-start(bf16[4,16,1024]{2,1,0:T(8,128)(2,1)} %broadcast_in_dim.16), calls=%async_computation | async-start | bytes 262144 | tf_op jit(solution)/shard_map/all_to_all | solution.py:11
  13.9 0.7 copy-start.5
  18.9 0.7 copy-start.7
  58.1 3.6 %copy-start.13 = (bf16[1024,4]{0,1:T(4,128)(2,1)S(1)}, bf16[1024,4]{0,1:T(4,128)(2,1)}, u32[]{:S(2)}) copy-start(bf16[1024,4]{0,1:T(4,128)(2,1)} %param.26) | copy-start | bytes 24580
  58.1 12.8 %all-to-all-start.2 = ((bf16[4,1,256,256]{2,3,1,0:T(8,128)(2,1)}), bf16[4,1,256,256]{2,3,1,0:T(8,128)(2,1)S(1)}, u32[]{:S(2)}, u32[]{:S(2)}) async-start(bf16[4,1,256,256]{2,3,1,0:T(8,128)(2,1)} %broadcast_in_dim.20), calls=%async_computation.2 | async-start | bytes 1048576 | tf_op jit(solution)/shard_map/all_to_all | solution.py:11
  70.8 1.0 copy-start.10
  73.2 3.6 %copy-start.4 = (bf16[1024,128]{1,0:T(8,128)(2,1)S(1)}, bf16[1024,128]{1,0:T(8,128)(2,1)}, u32[]{:S(2)}) copy-start(bf16[1024,128]{1,0:T(8,128)(2,1)} %param.27) | copy-start | bytes 786436
  73.2 11.6 %copy-start.11 = (bf16[1,1024,256]{2,1,0:T(8,128)(2,1)S(1)}, bf16[1,1024,256]{2,1,0:T(8,128)(2,1)}, u32[]{:S(2)}) copy-start(bf16[1,1024,256]{2,1,0:T(8,128)(2,1)} %param.31) | copy-start | bytes 1572868
  73.2 11.6 %all-to-all-start.3 = ((bf16[4,1,256,256]{2,3,1,0:T(8,128)(2,1)}), bf16[4,1,256,256]{2,3,1,0:T(8,128)(2,1)S(1)}, u32[]{:S(2)}, u32[]{:S(2)}) async-start(bf16[4,1,256,256]{2,3,1,0:T(8,128)(2,1)} %broadcast_in_dim.21), calls=%async_computation.3 | async-start | bytes 1048576 | tf_op jit(solution)/shard_map/all_to_all | solution.py:11
  88.0 24.8 %all-to-all-start.4 = ((bf16[128,2,256]{2,1,0:T(2,128)(2,1)}), bf16[128,2,256]{2,1,0:T(2,128)(2,1)S(1)}, u32[]{:S(2)}, u32[]{:S(2)}) async-start(bf16[128,2,256]{2,1,0:T(2,128)(2,1)} %reshape.224), calls=%async_computation.4 | async-start | bytes 262144 | tf_op jit(solution)/shard_map/all_to_all | solution.py:128
where the time goes:
time: 114 us
  blocking collectives  37.1 us (33%)
  waiting for transfers between devices  35.3 us (31%)
  starting transfers between devices  21 us (18%)
  local copies, waits for them, and re-layouts  8.1 us (7%)
  other arithmetic  7.64 us (7%)
  matrix products  3.55 us (3%)
    all_to_all x1, blocking collectives, local(): lax.all_to_all(outgoing, 'ep', split_axis=0, concat_axis=1, tiled=True)  37.1 us
    all_to_all x3, waiting for transfers between devices, from_everyone(): lax.all_to_all(jnp.broadcast_to(array[None], (count, *array.shape)), axis...  19.6 us
    all_to_all x1, waiting for transfers between devices, local(): lax.all_to_all(produced, 'ep', split_axis=1, concat_axis=0, tiled=True)  15.8 us
    all_to_all x3, starting transfers between devices, from_everyone(): lax.all_to_all(jnp.broadcast_to(array[None], (count, *array.shape)), axis...  12.2 us
    all_to_all x1, starting transfers between devices, local(): lax.all_to_all(produced, 'ep', split_axis=1, concat_axis=0, tiled=True)  8.82 us
    unnamed x32, local copies, waits for them, and re-layouts  4.59 us
    reduce_sum x1, other arithmetic, local(): readout = jnp.sum(new_state * query[..., None], axis=2)  2.85 us
    broadcast_in_dim x5, local copies, waits for them, and re-layouts, from_everyone(): jnp.broadcast_to(array[None], (count, *array.shape))  2.46 us
  transfers between devices with their start and end apart: 4, of which 4 were waited for; matrix products, arithmetic and copies ran while one was open for 2% of the time, Pallas kernels for 0%

commit v1 on v0

v1 whole, which is shorter than its diff:
```python
import jax
import jax.numpy as jnp
from jax import lax
from jax.experimental import pallas as pl
from jax.experimental.pallas import tpu as pltpu
from jax.sharding import PartitionSpec as P

epsilon = 1e-06
MESH = pl.DeviceIdType.MESH
BF = jnp.bfloat16
F32 = jnp.float32

DIST = [0] + [(p + 1) // 2 if p % 2 else 16 - p // 2 for p in range(1, 16)]
BACK = [DIST.index((16 - d) % 16) for d in DIST]
FAR = list(range(15, 0, -1))
CHUNKS = [(12, 16), (8, 12), (4, 8), (0, 4)]
GROUP = [j for j in (4, 5, 2, 3, 6, 7, 1)]


def group_back(j):
    return ((4 - j // 2) % 4) * 2 + j % 2


def kernel(
    tok_h,
    st_h,
    wq_h,
    wf_h,
    wi_h,
    lb_h,
    hg_h,
    wo_h,
    mg_h,
    fg_h,
    gw_h,
    ew_h,
    rt_h,
    wg_h,
    wu_h,
    wd_h,
    out_ref,
    ns_h,
    tok,
    st,
    wq,
    wf,
    wi,
    lb,
    hg,
    wo,
    mg,
    fg,
    gw,
    ew,
    rt,
    wg,
    wu,
    wd,
    hp,
    rs,
    d1,
    cb,
    res,
    gb,
    d2s,
    xb,
    hb,
    pb,
    rr,
    r2s,
    r2r,
    lsem,
    nsem,
    rs_s,
    rs_r,
    d1_s,
    d1_r,
    cb_s,
    cb_r,
    re_s,
    re_r,
    gb_s,
    gb_r,
    d2_s,
    d2_r,
    yf_s,
    yf_r,
    hb_s,
    hb_r,
    r1_s,
    r1_r,
    r2_ss,
    r2_rs,
    k1,
    k2,
    k3,
):
    e = lax.axis_index("ep")
    y = lax.axis_index("tp")
    c = lax.rem(e, 2)
    x = lax.rem(e // 2, 4)
    z = e // 8
    g = lax.rem(e, 8)

    def at_y(d):
        return (e, lax.rem(y + d, 4))

    def at_g(j):
        x2 = lax.rem(x + j // 2, 4)
        c2 = lax.rem(c + j % 2, 2)
        return ((z * 4 + x2) * 2 + c2, y)

    def at_z(d):
        return (lax.rem(z + d, 16) * 8 + g, y)

    def remote(src, dst, ss, sr, dev):
        return pltpu.make_async_remote_copy(
            src_ref=src, dst_ref=dst, send_sem=ss, recv_sem=sr, device_id=dev, device_id_type=MESH
        )

    barrier = pltpu.get_barrier_semaphore()
    for dev in [at_z(1), at_z(15)] + [at_g(j) for j in GROUP] + [at_y(d) for d in (2, 1, 3)]:
        pl.semaphore_signal(barrier, inc=1, device_id=dev, device_id_type=MESH)

    loads = {}
    pairs = [
        (tok_h, tok),
        (mg_h, mg),
        (wq_h, wq),
        (wf_h, wf),
        (wi_h, wi),
        (lb_h, lb),
        (st_h, st),
        (hg_h, hg),
        (wo_h, wo),
        (rt_h, rt),
        (fg_h, fg),
        (gw_h, gw),
        (ew_h, ew),
        (wg_h, wg),
        (wu_h, wu),
        (wd_h, wd),
    ]
    for i, (src, dst) in enumerate(pairs):
        loads[i] = pltpu.make_async_copy(src, dst, lsem.at[i])
        loads[i].start()

    sends = []

    for i in range(6):
        loads[i].wait()
    t32 = tok[...].astype(F32)
    normed = (
        t32 * lax.rsqrt(jnp.mean(t32 * t32, axis=-1, keepdims=True) + epsilon) * mg[...]
    ).astype(BF)
    q_pre = jnp.dot(normed, wq[...], preferred_element_type=F32)
    f_pre = jnp.dot(normed, wf[...], preferred_element_type=F32)
    value = jnp.dot(normed, wi[...], preferred_element_type=F32)
    query = q_pre * jax.nn.sigmoid(q_pre)
    forget = lb[...] + (1.0 - lb[...]) * jax.nn.sigmoid(f_pre)
    f_t = forget.T
    q_t = query.T
    loads[6].wait()
    rows = []
    for t in range(16):
        f_col = f_t[:, t : t + 1]
        new = f_col * st[t] + (1.0 - f_col) * value[t : t + 1, :]
        st[t] = new
        rows.append(jnp.sum(new * q_t[:, t : t + 1], axis=0, keepdims=True))
    new_copy = pltpu.make_async_copy(st, ns_h, nsem)
    new_copy.start()
    readout = jnp.concatenate(rows, axis=0)
    for i in range(7, 10):
        loads[i].wait()
    head_out = (
        readout
        * lax.rsqrt(jnp.mean(readout * readout, axis=-1, keepdims=True) + epsilon)
        * hg[...]
    ).astype(BF)
    part = jnp.dot(head_out, wo[...], preferred_element_type=F32).astype(BF)
    for b in range(4):
        hp[b] = part[:, b * 256 : (b + 1) * 256]

    lane = lax.broadcasted_iota(jnp.int32, (16, 128), 1)
    hits = jnp.zeros((16, 128), F32)
    routes = rt[...]
    for k in range(6):
        hits = hits + jnp.where(routes[:, k : k + 1] == lane, 1.0, 0.0)
    below = lax.broadcasted_iota(jnp.int32, (16, 16), 0) > lax.broadcasted_iota(
        jnp.int32, (16, 16), 1
    )
    before = jnp.dot(
        jnp.where(below, 1.0, 0.0).astype(BF), hits.astype(BF), preferred_element_type=F32
    )
    cb[0:16, :] = (hits * (1.0 + before)).astype(BF)

    pl.semaphore_wait(barrier, 12)
    for d in (1, 15):
        pl.semaphore_signal(k1, inc=1, device_id=at_z(d), device_id_type=MESH)

    for d in (2, 1, 3):
        to = lax.rem(y + d, 4)
        cp = remote(hp.at[to], rs.at[4 - d], rs_s.at[d], rs_r.at[4 - d], at_y(d))
        cp.start()
        sends.append(cp)
    own = slice(0, 16)
    for j in GROUP:
        b = group_back(j)
        cp = remote(cb.at[own], cb.at[pl.ds(b * 16, 16)], cb_s.at[j], cb_r.at[b], at_g(j))
        cp.start()
        sends.append(cp)
    pl.semaphore_wait(k1, 2)
    for d in (2, 14):
        pl.semaphore_signal(k2, inc=1, device_id=at_z(d), device_id_type=MESH)
    mixed = hp[y].astype(F32)
    for d in (1, 3, 2):
        remote(hp.at[0], rs.at[d], rs_s.at[d], rs_r.at[d], at_y(d)).wait_recv()
        mixed = mixed + rs[d].astype(F32)
    resident = tok[:, pl.ds(pl.multiple_of(y * 256, 256), 256)].astype(F32)
    resid = (resident + mixed.astype(BF).astype(F32)).astype(BF)
    d1[own, :] = resid

    for j in GROUP:
        b = group_back(j)
        cp = remote(d1.at[own], d1.at[pl.ds(b * 16, 16)], d1_s.at[j], d1_r.at[b], at_g(j))
        cp.start()
        sends.append(cp)
    res[y] = resid
    for d in (2, 1, 3):
        cp = remote(d1.at[own], res.at[y], re_s.at[d], re_r.at[4 - d], at_y(d))
        cp.start()
        sends.append(cp)

    def blocks(shape, axis):
        index = lax.broadcasted_iota(jnp.int32, shape, axis)
        p = lax.shift_right_logical(index, 4)
        half = lax.shift_right_logical(p, 1)
        dist = jnp.where((p & 1) == 1, half + 1, (16 - half) & 15)
        expert = ((z + dist) & 15) * 8 + g
        return expert, lax.shift_right_logical(index, 1) & 7, (index & 1).astype(F32) + 1.0

    expert, source, want = blocks((256, 128), 0)
    along = lax.broadcasted_iota(jnp.int32, (256, 128), 1)
    sel = jnp.where(expert == along, 1.0, 0.0).astype(BF)
    for j in range(1, 8):
        remote(
            cb.at[own], cb.at[pl.ds(j * 16, 16)], cb_s.at[j], cb_r.at[j], at_g(j)
        ).wait_recv()
    codes = cb[...]
    nt = (((1,), (1,)), ((), ()))
    found = lax.dot_general(sel, codes, nt, preferred_element_type=F32)
    spread = jnp.where(
        (found == want) & (source == lax.shift_right_logical(along, 4)), 1.0, 0.0
    ).astype(BF)
    pl.semaphore_wait(k2, 2)
    for d in (4, 12):
        pl.semaphore_signal(k3, inc=1, device_id=at_z(d), device_id_type=MESH)
    for j in range(1, 8):
        remote(
            d1.at[own], d1.at[pl.ds(j * 16, 16)], d1_s.at[j], d1_r.at[j], at_g(j)
        ).wait_recv()
    d2s[...] = jnp.dot(spread, d1[...], preferred_element_type=F32).astype(BF)
    pl.semaphore_wait(k3, 2)

    def rows_of(p):
        return pl.ds(p * 16, 16)

    for p in FAR:
        cp = remote(
            d2s.at[rows_of(p)],
            xb.at[y, rows_of(BACK[p])],
            d2_s.at[p],
            d2_r.at[BACK[p]],
            at_z(DIST[p]),
        )
        cp.start()
        sends.append(cp)
    xb[y, 0:16, :] = d2s[0:16, :]

    def forward(p):
        for d in (2, 1, 3):
            cp = remote(
                xb.at[y, rows_of(p)],
                xb.at[y, rows_of(p)],
                yf_s.at[p * 4 + d],
                yf_r.at[p * 4 + 4 - d],
                at_y(d),
            )
            cp.start()
            sends.append(cp)

    forward(0)

    for d in (1, 3, 2):
        remote(
            d1.at[own], res.at[lax.rem(y + d, 4)], re_s.at[d], re_r.at[d], at_y(d)
        ).wait_recv()
    for i in range(10, 13):
        loads[i].wait()
    gain = fg[...]
    r32 = jnp.concatenate([res[b] for b in range(4)], axis=1).astype(F32)
    ffn_in = (
        r32 * lax.rsqrt(jnp.mean(r32 * r32, axis=-1, keepdims=True) + epsilon) * gain
    ).astype(BF)
    group_raw = jnp.exp(jnp.dot(ffn_in, gw[...], preferred_element_type=F32))
    group_prob = group_raw / jnp.sum(group_raw, axis=-1, keepdims=True)
    raw = jnp.exp(jnp.dot(ffn_in, ew[...], preferred_element_type=F32))
    member = lax.shift_right_logical(lane, 5)
    total = jnp.zeros((16, 128), F32)
    prior = jnp.zeros((16, 128), F32)
    for k in range(4):
        mine = member == k
        total = jnp.where(
            mine, jnp.sum(jnp.where(mine, raw, 0.0), axis=-1, keepdims=True), total
        )
        prior = jnp.where(mine, group_prob[:, k : k + 1], prior)
    weight = jnp.where(hits > 0.0, raw / total * prior, 0.0)
    gate = weight / jnp.sum(weight, axis=-1, keepdims=True)
    gate_hi = gate.astype(BF)
    gb[0, 0:16, :] = gate_hi
    gb[1, 0:16, :] = (gate - gate_hi.astype(F32)).astype(BF)
    for j in GROUP:
        b = group_back(j)
        cp = remote(
            gb.at[:, own], gb.at[:, pl.ds(b * 16, 16)], gb_s.at[j], gb_r.at[b], at_g(j)
        )
        cp.start()
        sends.append(cp)

    for p in FAR:
        remote(
            d2s.at[rows_of(p)], xb.at[y, rows_of(p)], d2_s.at[p], d2_r.at[p], at_z(DIST[p])
        ).wait_recv()
        forward(p)

    for i in range(13, 16):
        loads[i].wait()

    def wait_rows(lo, hi):
        for p in range(lo, hi):
            for d in (1, 3, 2):
                at = xb.at[lax.rem(y + d, 4), rows_of(p)]
                remote(at, at, yf_s.at[p * 4 + d], yf_r.at[p * 4 + d], at_y(d)).wait_recv()

    for n, (lo, hi) in enumerate(CHUNKS):
        wait_rows(lo, hi)
        span = slice(lo * 16, hi * 16)
        a32 = jnp.concatenate([xb[b, span, :] for b in range(4)], axis=1).astype(F32)
        rows_in = (
            a32 * lax.rsqrt(jnp.mean(a32 * a32, axis=-1, keepdims=True) + epsilon) * gain
        ).astype(BF)
        gate_hidden = jnp.dot(rows_in, wg[...], preferred_element_type=F32)
        up_hidden = jnp.dot(rows_in, wu[...], preferred_element_type=F32)
        hb[y, span, :] = (gate_hidden * jax.nn.sigmoid(gate_hidden) * up_hidden).astype(BF)
        for d in (2, 1, 3):
            cp = remote(
                hb.at[y, span],
                hb.at[y, span],
                hb_s.at[n * 4 + d],
                hb_r.at[n * 4 + 4 - d],
                at_y(d),
            )
            cp.start()
            sends.append(cp)

    for j in range(1, 8):
        remote(
            gb.at[:, own], gb.at[:, pl.ds(j * 16, 16)], gb_s.at[j], gb_r.at[j], at_g(j)
        ).wait_recv()
    _, source_t, want_t = blocks((128, 256), 1)
    token_t = lax.shift_right_logical(lax.broadcasted_iota(jnp.int32, (128, 256), 0), 4)
    found_t = lax.dot_general(codes, sel, nt, preferred_element_type=F32)
    here = (found_t == want_t) & (source_t == token_t)
    mix_hi = jnp.where(
        here, lax.dot_general(gb[0], sel, nt, preferred_element_type=F32), 0.0
    ).astype(BF)
    mix_lo = jnp.where(
        here, lax.dot_general(gb[1], sel, nt, preferred_element_type=F32), 0.0
    ).astype(BF)

    for n, (lo, hi) in enumerate(CHUNKS):
        span = slice(lo * 16, hi * 16)
        for d in (1, 3, 2):
            at = hb.at[lax.rem(y + d, 4), span]
            remote(at, at, hb_s.at[n * 4 + d], hb_r.at[n * 4 + d], at_y(d)).wait_recv()
        hidden = jnp.concatenate([hb[b, span, :] for b in range(4)], axis=1)
        pb[span, :] = jnp.dot(hidden, wd[...], preferred_element_type=F32).astype(BF)
        for p in range(hi - 1, lo - 1, -1):
            if p:
                cp = remote(
                    pb.at[rows_of(p)],
                    rr.at[rows_of(BACK[p])],
                    r1_s.at[p],
                    r1_r.at[BACK[p]],
                    at_z(DIST[p]),
                )
                cp.start()
                sends.append(cp)
    rr[0:16, :] = pb[0:16, :]

    for p in range(1, 16):
        remote(
            pb.at[rows_of(p)], rr.at[rows_of(p)], r1_s.at[p], r1_r.at[p], at_z(DIST[p])
        ).wait_recv()
    back = rr[...]
    sums = jnp.dot(mix_hi, back, preferred_element_type=F32) + jnp.dot(
        mix_lo, back, preferred_element_type=F32
    )
    r2s[...] = sums.astype(BF)
    for j in GROUP:
        b = group_back(j)
        cp = remote(
            r2s.at[pl.ds(j * 16, 16)], r2r.at[pl.ds(b * 16, 16)], r2_ss.at[j], r2_rs.at[b], at_g(j)
        )
        cp.start()
        sends.append(cp)
    mixture = sums[0:16, :]
    for j in range(1, 8):
        remote(
            r2s.at[pl.ds(j * 16, 16)], r2r.at[pl.ds(j * 16, 16)], r2_ss.at[j], r2_rs.at[j], at_g(j)
        ).wait_recv()
        mixture = mixture + r2r[j * 16 : (j + 1) * 16, :].astype(F32)
    out_ref[...] = (d1[own, :].astype(F32) + mixture).astype(BF)
    new_copy.wait()
    for cp in sends:
        cp.wait_send()


def local(
    tokens,
    old_state,
    query_weight,
    forget_weight,
    input_weight,
    lower_bound,
    head_gain,
    out_weight,
    mix_gain,
    ffn_gain,
    group_weight,
    expert_weight,
    routes,
    gate_weight,
    up_weight,
    down_weight,
):
    operands = (
        tokens,
        old_state.reshape(16, 128, 128),
        query_weight,
        forget_weight,
        input_weight,
        lower_bound.reshape(1, 128),
        head_gain,
        out_weight,
        mix_gain.reshape(1, 1024),
        ffn_gain.reshape(1, 1024),
        group_weight,
        expert_weight,
        routes,
        gate_weight.reshape(1024, 256),
        up_weight.reshape(1024, 256),
        down_weight.reshape(1024, 256),
    )
    dma = pltpu.SemaphoreType.DMA
    layer_out, new_state = pl.pallas_call(
        kernel,
        name="layer",
        out_shape=(
            jax.ShapeDtypeStruct((16, 256), BF),
            jax.ShapeDtypeStruct((16, 128, 128), F32),
        ),
        in_specs=[pl.BlockSpec(memory_space=pl.ANY)] * 16,
        out_specs=(pl.BlockSpec(memory_space=pltpu.VMEM), pl.BlockSpec(memory_space=pl.ANY)),
        scratch_shapes=[pltpu.VMEM(a.shape, a.dtype) for a in operands]
        + [
            pltpu.VMEM((4, 16, 256), BF),
            pltpu.VMEM((4, 16, 256), BF),
            pltpu.VMEM((128, 256), BF),
            pltpu.VMEM((128, 128), BF),
            pltpu.VMEM((4, 16, 256), BF),
            pltpu.VMEM((2, 128, 128), BF),
            pltpu.VMEM((256, 256), BF),
            pltpu.VMEM((4, 256, 256), BF),
            pltpu.VMEM((4, 256, 256), BF),
            pltpu.VMEM((256, 256), BF),
            pltpu.VMEM((256, 256), BF),
            pltpu.VMEM((128, 256), BF),
            pltpu.VMEM((128, 256), BF),
            dma((16,)),
            dma(()),
        ]
        + [dma((4,))] * 2
        + [dma((8,))] * 4
        + [dma((4,))] * 2
        + [dma((8,))] * 2
        + [dma((16,))] * 2
        + [dma((64,))] * 2
        + [dma((16,))] * 2
        + [dma((16,))] * 2
        + [dma((8,))] * 2
        + [pltpu.SemaphoreType.REGULAR] * 3,
        compiler_params=pltpu.CompilerParams(collective_id=0, has_side_effects=True),
    )(*operands)
    return layer_out, new_state.reshape(16, 1, 128, 128)


def solution(mesh):
    in_specs = (
        P("ep", None),
        P("ep", "tp", None, None),
        P(None, "tp"),
        P(None, "tp"),
        P(None, "tp"),
        P("tp"),
        P("tp", None),
        P("tp", None),
        P(),
        P(),
        P(),
        P(),
        P("ep", None),
        P("ep", None, "tp"),
        P("ep", None, "tp"),
        P("ep", None, "tp"),
    )
    out_specs = (P("ep", "tp"), P("ep", "tp", None, None))
    return jax.shard_map(local, mesh=mesh, in_specs=in_specs, out_specs=out_specs, check_vma=False)
```

time: 114 us -> 61.2 us (0.54)
  Pallas kernels: 0 us -> 54.5 us
  blocking collectives: 37.1 us -> 0 us
  waiting for transfers between devices: 35.3 us -> 0 us
  starting transfers between devices: 21 us -> 0 us
  other arithmetic: 7.64 us -> 0 us
  matrix products: 3.55 us -> 0 us
  local copies, waits for them, and re-layouts: 8.1 us -> 5.82 us
    pallas_call x0 -> x1, Pallas kernels: none -> 54.5 us  [local(): pl.pallas_call(kernel, name='layer', out_shape=(jax.ShapeDtypeStruct((16,...]
    all_to_all x1 -> x0, blocking collectives: 37.1 us -> none  [local(): lax.all_to_all(outgoing, 'ep', split_axis=0, concat_axis=1, tiled=True)]
    all_to_all x4 -> x0, waiting for transfers between devices: 35.3 us -> none  [the longest x3 19.6 us: from_everyone(): lax.all_to_all(jnp.broadcast_to(array[None], (count, *array.shape)), axis...]
    all_to_all x4 -> x0, starting transfers between devices: 21 us -> none  [the longest x3 12.2 us: from_everyone(): lax.all_to_all(jnp.broadcast_to(array[None], (count, *array.shape)), axis...]
    reduce_sum x8 -> x0, other arithmetic: 4.53 us -> none  [the longest x1 2.85 us: local(): readout = jnp.sum(new_state * query[..., None], axis=2)]
    dot_general x11 -> x0, matrix products: 3.55 us -> none  [the longest x1 1.2 us: local(): jnp.dot(normed, query_weight, preferred_element_type=jnp.float32)]
    broadcast_in_dim x5 -> x0, local copies, waits for them, and re-layouts: 2.46 us -> none  [from_everyone(): jnp.broadcast_to(array[None], (count, *array.shape))]
    unnamed x1 -> x0, other arithmetic: 1.41 us -> none
  transfers between devices with their start and end apart: 4 -> 0, of which waited for: 4 -> 0; matrix products, arithmetic and copies ran while one was open for 2% -> 0% of each run, Pallas kernels for 0% -> 0%
where the time goes in v1:
time: 61.2 us; the launch traced here: 61 us
  Pallas kernels  54.5 us (89%)
  local copies, waits for them, and re-layouts  5.82 us (10%)
  between operations  0.66 us (1%)
    pallas_call x1, Pallas kernels, local(): pl.pallas_call(kernel, name='layer', out_shape=(jax.ShapeDtypeStruct((16,...  54.5 us
    unnamed x8, local copies, waits for them, and re-layouts  5.82 us

profile of v1, /device:TPU:1, one launch (start us, length us, event | category | flops | bytes accessed | tf_op | source)
XLA Modules:
  0.0 61.0 jit_solution(10867711022428211006)
XLA Ops:
  0.6 0.0 copy-start.1
  0.6 0.0 copy-start
  0.6 0.7 %copy-done.1 = s32[16,6]{0,1:T(8,128)S(1)} copy-done((s32[16,6]{0,1:T(8,128)S(1)}, s32[16,6]{0,1:T(8,128)}, u32[]{:S(2)}) %copy-start.1) | copy-done | bytes 408
  1.3 0.7 %copy.19.rt_h = s32[16,6]{1,0:T(8,128)} copy(s32[16,6]{0,1:T(8,128)S(1)} %copy-done.1) | data formatting | bytes 768 | tf_op args[12]
  2.0 0.0 copy-done
  2.0 0.9 %copy.18.gw_h = bf16[1024,4]{1,0:T(8,128)(2,1)} copy(bf16[1024,4]{0,1:T(4,128)(2,1)S(1)} %copy-done) | data formatting | bytes 16384 | tf_op args[10]
  2.9 54.5 %layer.1 = (bf16[16,256]{1,0:T(8,128)(2,1)}, f32[16,128,128]{2,1,0:T(8,128)}) custom-call(bf16[16,1024]{1,0:T(8,128)(2,1)} %tok_h.1, f32[16,128,128]{2,1,0:T(8,128)} %bitcast.10, bf16[1024,128]{1,0:T(8,128)(2,1)} %wq_h.1, bf16[1024,128]{1,0:T(8,128)(2,1)} %wf_h.1, bf16[1024,128]{1,0:T(8,128)(2,1)} %wi_h.1, f32[1,128]{1,0:T(1,128)} %bitcast.17, ...), custom_call_target="tpu_custom_call" | custom-call | tf_op jit(solution)/shard_map/layer/pallas_call | solution.py:466
  57.4 1.3 %copy.23 = bf16[16,256]{1,0:T(8,128)(2,1)} copy(bf16[16,256]{1,0:T(8,128)(2,1)} %get-tuple-element.10) | data formatting | bytes 16384
  58.7 2.3 %copy.24 = f32[16,1,128,128]{3,2,1,0:T(8,128)} copy(f32[16,1,128,128]{3,2,1,0:T(8,128)} %bitcast.11) | data formatting | bytes 2097152
Async XLA Ops:
  0.6 0.7 %copy-start.1 = (s32[16,6]{0,1:T(8,128)S(1)}, s32[16,6]{0,1:T(8,128)}, u32[]{:S(2)}) copy-start(s32[16,6]{0,1:T(8,128)} %param.28) | copy-start | bytes 1156
  0.6 1.4 %copy-start = (bf16[1024,4]{0,1:T(4,128)(2,1)S(1)}, bf16[1024,4]{0,1:T(4,128)(2,1)}, u32[]{:S(2)}) copy-start(bf16[1024,4]{0,1:T(4,128)(2,1)} %param.26) | copy-start | bytes 24580

commit v2 on v1

v2 whole, which is shorter than its diff:
```python
import jax
import jax.numpy as jnp
from jax import lax
from jax.experimental import pallas as pl
from jax.experimental.pallas import tpu as pltpu
from jax.sharding import PartitionSpec as P

epsilon = 1e-06
MESH = pl.DeviceIdType.MESH
BF = jnp.bfloat16
F32 = jnp.float32

DIST = [0] + [(p + 1) // 2 if p % 2 else 16 - p // 2 for p in range(1, 16)]
BACK = [DIST.index((16 - d) % 16) for d in DIST]
FAR = list(range(15, 0, -1))
ARRIVE = [8, 7, 6, 5, 4, 3, 2, 1, 0, 15, 14, 13, 12, 11, 10, 9]
CHUNKS = [(4, 9), (0, 4), (13, 16), (9, 13)]
GROUP = [4, 5, 2, 3, 6, 7, 1]


def hops(p, j):
    return min(DIST[p], 16 - DIST[p]) + min(j // 2, 4 - j // 2)


ORDER = sorted(
    [(p, j) for p in range(16) for j in range(8) if p or j], key=lambda at: -hops(*at)
)


def group_back(j):
    return ((4 - j // 2) % 4) * 2 + j % 2


def kernel(
    tok_h,
    st_h,
    wq_h,
    wf_h,
    wi_h,
    lb_h,
    hg_h,
    wo_h,
    mg_h,
    fg_h,
    gw_h,
    ew_h,
    rt_h,
    wg_h,
    wu_h,
    wd_h,
    out_ref,
    ns_ref,
    tok,
    st,
    wq,
    wf,
    wi,
    lb,
    hg,
    wo,
    mg,
    fg,
    gw,
    ew,
    rt,
    wg,
    wu,
    wd,
    hp,
    rs,
    d1,
    res,
    d2s,
    xb,
    hb,
    pb,
    rr,
    lsem,
    rs_s,
    rs_r,
    re_s,
    re_r,
    d2_s,
    d2_r,
    yf_s,
    yf_r,
    hb_s,
    hb_r,
    r1_s,
    r1_r,
    k1,
    k2,
):
    e = lax.axis_index("ep")
    y = lax.axis_index("tp")
    c = lax.rem(e, 2)
    x = lax.rem(e // 2, 4)
    z = e // 8
    g = lax.rem(e, 8)

    def at_y(d):
        return (e, lax.rem(y + d, 4))

    def at_g(j):
        x2 = lax.rem(x + j // 2, 4)
        c2 = lax.rem(c + j % 2, 2)
        return ((z * 4 + x2) * 2 + c2, y)

    def at_z(d):
        return (lax.rem(z + d, 16) * 8 + g, y)

    def remote(src, dst, ss, sr, dev):
        return pltpu.make_async_remote_copy(
            src_ref=src, dst_ref=dst, send_sem=ss, recv_sem=sr, device_id=dev, device_id_type=MESH
        )

    barrier = pltpu.get_barrier_semaphore()
    first = [at_z(d) for d in (4, 12, 3, 13, 2, 14, 1, 15)]
    first += [at_g(j) for j in GROUP] + [at_y(d) for d in (2, 1, 3)]
    for dev in first:
        pl.semaphore_signal(barrier, inc=1, device_id=dev, device_id_type=MESH)

    loads = {}
    pairs = [
        (tok_h, tok),
        (mg_h, mg),
        (wq_h, wq),
        (wf_h, wf),
        (wi_h, wi),
        (lb_h, lb),
        (st_h, st),
        (hg_h, hg),
        (wo_h, wo),
        (rt_h, rt),
        (fg_h, fg),
        (gw_h, gw),
        (ew_h, ew),
        (wg_h, wg),
        (wu_h, wu),
        (wd_h, wd),
    ]
    for i, (src, dst) in enumerate(pairs):
        loads[i] = pltpu.make_async_copy(src, dst, lsem.at[i])
        loads[i].start()

    sends = []
    due = {}

    def post(key, src, dst, ss, sr, dev, arriving, own_ss, own_sr):
        cp = remote(src, dst, ss, sr, dev)
        cp.start()
        sends.append(cp)
        due[key] = remote(src, arriving, own_ss, own_sr, dev)

    def got(key):
        due.pop(key).wait_recv()

    for i in range(6):
        loads[i].wait()
    t32 = tok[...].astype(F32)
    normed = (
        t32 * lax.rsqrt(jnp.mean(t32 * t32, axis=-1, keepdims=True) + epsilon) * mg[...]
    ).astype(BF)
    q_pre = jnp.dot(normed, wq[...], preferred_element_type=F32)
    f_pre = jnp.dot(normed, wf[...], preferred_element_type=F32)
    value = jnp.dot(normed, wi[...], preferred_element_type=F32)
    query = q_pre * jax.nn.sigmoid(q_pre)
    forget = lb[...] + (1.0 - lb[...]) * jax.nn.sigmoid(f_pre)
    f_t = forget.T
    q_t = query.T
    loads[6].wait()
    rows = []
    for t in range(16):
        f_col = f_t[:, t : t + 1]
        new = f_col * st[t] + (1.0 - f_col) * value[t : t + 1, :]
        ns_ref[t] = new
        rows.append(jnp.sum(new * q_t[:, t : t + 1], axis=0, keepdims=True))
    readout = jnp.concatenate(rows, axis=0)
    for i in range(7, 10):
        loads[i].wait()
    head_out = (
        readout
        * lax.rsqrt(jnp.mean(readout * readout, axis=-1, keepdims=True) + epsilon)
        * hg[...]
    ).astype(BF)
    part = jnp.dot(head_out, wo[...], preferred_element_type=F32).astype(BF)
    for b in range(4):
        hp[b] = part[:, b * 256 : (b + 1) * 256]

    lane = lax.broadcasted_iota(jnp.int32, (16, 128), 1)
    nt = (((1,), (1,)), ((), ()))
    down = lax.broadcasted_iota(jnp.int32, (128, 16), 0)
    named = jnp.zeros((128, 16), F32)
    routes = rt[...]
    for k in range(6):
        named = named + jnp.where(routes[k : k + 1, :] == down, 1.0, 0.0)
    named = named.astype(BF)
    row = lax.broadcasted_iota(jnp.int32, (16, 16), 0)
    col = lax.broadcasted_iota(jnp.int32, (16, 16), 1)
    same = jnp.where(row == col, 1.0, 0.0).astype(BF)
    below = jnp.where(row > col, 1.0, 0.0).astype(BF)
    hits = lax.dot_general(same, named, nt, preferred_element_type=F32)
    before = lax.dot_general(below, named, nt, preferred_element_type=F32)
    codes = (hits * (1.0 + before)).astype(BF)

    def blocks(shape, axis):
        index = lax.broadcasted_iota(jnp.int32, shape, axis)
        p = lax.shift_right_logical(index, 4)
        half = lax.shift_right_logical(p, 1)
        dist = jnp.where((p & 1) == 1, half + 1, (16 - half) & 15)
        j = lax.shift_right_logical(index, 1) & 7
        there = ((x + lax.shift_right_logical(j, 1)) & 3) * 2 + ((c + j) & 1)
        return ((z + dist) & 15) * 8 + there, (index & 1).astype(F32) + 1.0

    expert, _ = blocks((256, 128), 0)
    along = lax.broadcasted_iota(jnp.int32, (256, 128), 1)
    sel = jnp.where(expert == along, 1.0, 0.0).astype(BF)
    _, want = blocks((256, 16), 0)
    found = lax.dot_general(sel, codes, nt, preferred_element_type=F32)
    spread = jnp.where(found == want, 1.0, 0.0).astype(BF)

    pl.semaphore_wait(barrier, 18)
    for j in GROUP:
        pl.semaphore_signal(k1, inc=1, device_id=at_g(j), device_id_type=MESH)

    for d in (2, 1, 3):
        to = lax.rem(y + d, 4)
        post(
            ("rs", d), hp.at[to], rs.at[4 - d], rs_s.at[d], rs_r.at[4 - d], at_y(d),
            rs.at[d], rs_s.at[d], rs_r.at[d],
        )
    pl.semaphore_wait(k1, 7)
    for d in (4, 12):
        pl.semaphore_signal(k2, inc=1, device_id=at_z(d), device_id_type=MESH)
    mixed = hp[y].astype(F32)
    for d in (1, 3, 2):
        got(("rs", d))
        mixed = mixed + rs[d].astype(F32)
    resident = tok[:, pl.ds(pl.multiple_of(y * 256, 256), 256)].astype(F32)
    resid = (resident + mixed.astype(BF).astype(F32)).astype(BF)
    d1[...] = resid
    d2s[...] = jnp.dot(spread, resid, preferred_element_type=F32).astype(BF)

    def rows_of(p):
        return pl.ds(p * 16, 16)

    def pair(p, j):
        return pl.ds(p * 16 + j * 2, 2)

    def block(p):
        return pl.ds(p * 16, 16)

    def sem(p, j):
        return p if p else 16 + j

    def at(p, j):
        x2 = lax.rem(x + j // 2, 4)
        c2 = lax.rem(c + j % 2, 2)
        return ((lax.rem(z + DIST[p], 16) * 4 + x2) * 2 + c2, y)

    for at_far in (False, True):
      if at_far:
        pl.semaphore_wait(k2, 2)
      for p, j in [o for o in ORDER if (o[0] > 8) == at_far]:
        remote(
            d2s.at[pair(p, j)],
            xb.at[y, pair(BACK[p], group_back(j))],
            d2_s.at[sem(p, j)],
            d2_r.at[sem(BACK[p], group_back(j))],
            at(p, j),
        ).start()
    for p, j in [(0, j) for j in range(1, 8)] + [(p, 0) for p in range(1, 16)]:
        span = block(p) if p else pair(p, j)
        both = remote(
            d2s.at[span], xb.at[y, span], d2_s.at[sem(p, j)], d2_r.at[sem(p, j)], at(p, j)
        )
        sends.append(both)
        due[("d2", p, j)] = both
    xb[y, 0:2, :] = d2s[0:2, :]

    def forward(p):
        for d in (2, 1, 3):
            post(
                ("yf", p, d), xb.at[y, rows_of(p)], xb.at[y, rows_of(p)],
                yf_s.at[p * 4 + d], yf_r.at[p * 4 + 4 - d], at_y(d),
                xb.at[lax.rem(y + d, 4), rows_of(p)], yf_s.at[p * 4 + d], yf_r.at[p * 4 + d],
            )

    for p in ARRIVE:
        for j in range(1, 8) if p == 0 else (0,):
            got(("d2", p, j))
        forward(p)

    for d in (2, 1, 3):
        post(
            ("re", d), d1, res.at[y], re_s.at[d], re_r.at[4 - d], at_y(d),
            res.at[lax.rem(y + d, 4)], re_s.at[d], re_r.at[d],
        )
    res[y] = resid

    for i in range(10, 13):
        loads[i].wait()
    gain = fg[...]
    for i in range(13, 16):
        loads[i].wait()

    def wait_rows(lo, hi):
        for p in range(lo, hi):
            for d in (1, 3, 2):
                got(("yf", p, d))

    for n, (lo, hi) in enumerate(CHUNKS):
        wait_rows(lo, hi)
        span = slice(lo * 16, hi * 16)
        a32 = jnp.concatenate([xb[b, span, :] for b in range(4)], axis=1).astype(F32)
        rows_in = (
            a32 * lax.rsqrt(jnp.mean(a32 * a32, axis=-1, keepdims=True) + epsilon) * gain
        ).astype(BF)
        gate_hidden = jnp.dot(rows_in, wg[...], preferred_element_type=F32)
        up_hidden = jnp.dot(rows_in, wu[...], preferred_element_type=F32)
        hb[y, span, :] = (gate_hidden * jax.nn.sigmoid(gate_hidden) * up_hidden).astype(BF)
        for d in (2, 1, 3):
            post(
                ("hb", n, d), hb.at[y, span], hb.at[y, span],
                hb_s.at[n * 4 + d], hb_r.at[n * 4 + 4 - d], at_y(d),
                hb.at[lax.rem(y + d, 4), span], hb_s.at[n * 4 + d], hb_r.at[n * 4 + d],
            )

    for n, (lo, hi) in enumerate(CHUNKS):
        span = slice(lo * 16, hi * 16)
        for d in (1, 3, 2):
            got(("hb", n, d))
        hidden = jnp.concatenate([hb[b, span, :] for b in range(4)], axis=1)
        pb[span, :] = jnp.dot(hidden, wd[...], preferred_element_type=F32).astype(BF)
        for p in range(hi - 1, lo - 1, -1):
            for j in (4, 5, 2, 3, 6, 7, 1, 0):
                if p or j:
                    remote(
                        pb.at[pair(p, j)],
                        rr.at[pair(BACK[p], group_back(j))],
                        r1_s.at[sem(p, j)],
                        r1_r.at[sem(BACK[p], group_back(j))],
                        at(p, j),
                    ).start()
    rr[0:2, :] = pb[0:2, :]
    for p, j in [(0, j) for j in range(1, 8)] + [(p, 0) for p in range(1, 16)]:
        span = block(p) if p else pair(p, j)
        both = remote(
            pb.at[span], rr.at[span], r1_s.at[sem(p, j)], r1_r.at[sem(p, j)], at(p, j)
        )
        sends.append(both)
        due[("r1", p, j)] = both

    for d in (1, 3, 2):
        got(("re", d))
    r32 = jnp.concatenate([res[b] for b in range(4)], axis=1).astype(F32)
    ffn_in = (
        r32 * lax.rsqrt(jnp.mean(r32 * r32, axis=-1, keepdims=True) + epsilon) * gain
    ).astype(BF)
    group_raw = jnp.exp(lax.dot_general(ffn_in, gw[...], nt, preferred_element_type=F32))
    group_prob = group_raw / jnp.sum(group_raw, axis=-1, keepdims=True)
    raw = jnp.exp(jnp.dot(ffn_in, ew[...], preferred_element_type=F32))
    member = lax.shift_right_logical(lane, 5)
    total = jnp.zeros((16, 128), F32)
    prior = jnp.zeros((16, 128), F32)
    for k in range(4):
        mine = member == k
        total = jnp.where(
            mine, jnp.sum(jnp.where(mine, raw, 0.0), axis=-1, keepdims=True), total
        )
        prior = jnp.where(mine, group_prob[:, k : k + 1], prior)
    weight = jnp.where(hits > 0.0, raw / total * prior, 0.0)
    gate = weight / jnp.sum(weight, axis=-1, keepdims=True)
    gate_hi = gate.astype(BF)
    gate_lo = (gate - gate_hi.astype(F32)).astype(BF)
    _, want_t = blocks((16, 256), 1)
    here = lax.dot_general(codes, sel, nt, preferred_element_type=F32) == want_t
    mix_hi = jnp.where(
        here, lax.dot_general(gate_hi, sel, nt, preferred_element_type=F32), 0.0
    ).astype(BF)
    mix_lo = jnp.where(
        here, lax.dot_general(gate_lo, sel, nt, preferred_element_type=F32), 0.0
    ).astype(BF)

    for p in range(16):
        for j in range(1, 8) if p == 0 else (0,):
            got(("r1", p, j))
    back = rr[...]
    mixture = jnp.dot(mix_hi, back, preferred_element_type=F32) + jnp.dot(
        mix_lo, back, preferred_element_type=F32
    )
    out_ref[...] = (d1[...].astype(F32) + mixture).astype(BF)
    for cp in sends:
        cp.wait_send()


def local(
    tokens,
    old_state,
    query_weight,
    forget_weight,
    input_weight,
    lower_bound,
    head_gain,
    out_weight,
    mix_gain,
    ffn_gain,
    group_weight,
    expert_weight,
    routes,
    gate_weight,
    up_weight,
    down_weight,
):
    operands = (
        tokens,
        old_state.reshape(16, 128, 128),
        query_weight,
        forget_weight,
        input_weight,
        lower_bound.reshape(1, 128),
        head_gain,
        out_weight,
        mix_gain.reshape(1, 1024),
        ffn_gain.reshape(1, 1024),
        group_weight.T,
        expert_weight,
        routes.T,
        gate_weight.reshape(1024, 256),
        up_weight.reshape(1024, 256),
        down_weight.reshape(1024, 256),
    )
    operands = [pltpu.with_memory_space_constraint(a, pltpu.HBM) for a in operands]
    dma = pltpu.SemaphoreType.DMA
    layer_out, new_state = pl.pallas_call(
        kernel,
        name="layer",
        out_shape=(
            jax.ShapeDtypeStruct((16, 256), BF),
            jax.ShapeDtypeStruct((16, 128, 128), F32),
        ),
        in_specs=[pl.BlockSpec(memory_space=pltpu.HBM)] * 16,
        out_specs=(pl.BlockSpec(memory_space=pltpu.VMEM),) * 2,
        scratch_shapes=[pltpu.VMEM(a.shape, a.dtype) for a in operands]
        + [
            pltpu.VMEM((4, 16, 256), BF),
            pltpu.VMEM((4, 16, 256), BF),
            pltpu.VMEM((16, 256), BF),
            pltpu.VMEM((4, 16, 256), BF),
            pltpu.VMEM((256, 256), BF),
            pltpu.VMEM((4, 256, 256), BF),
            pltpu.VMEM((4, 256, 256), BF),
            pltpu.VMEM((256, 256), BF),
            pltpu.VMEM((256, 256), BF),
            dma((16,)),
        ]
        + [dma((4,))] * 4
        + [dma((24,))] * 2
        + [dma((64,))] * 2
        + [dma((16,))] * 2
        + [dma((24,))] * 2
        + [pltpu.SemaphoreType.REGULAR] * 2,
        compiler_params=pltpu.CompilerParams(collective_id=0, has_side_effects=True, vmem_limit_bytes=16 * 1024 * 1024),
    )(*operands)
    return layer_out, new_state.reshape(16, 1, 128, 128)


def solution(mesh):
    in_specs = (
        P("ep", None),
        P("ep", "tp", None, None),
        P(None, "tp"),
        P(None, "tp"),
        P(None, "tp"),
        P("tp"),
        P("tp", None),
        P("tp", None),
        P(),
        P(),
        P(),
        P(),
        P("ep", None),
        P("ep", None, "tp"),
        P("ep", None, "tp"),
        P("ep", None, "tp"),
    )
    out_specs = (P("ep", "tp"), P("ep", "tp", None, None))
    return jax.shard_map(local, mesh=mesh, in_specs=in_specs, out_specs=out_specs, check_vma=False)
```

time: 61.2 us -> 54 us (0.88)
  local copies, waits for them, and re-layouts: 5.82 us -> 1.57 us
  Pallas kernels: 54.5 us -> 51.6 us
    unnamed x8 -> x2, local copies, waits for them, and re-layouts: 5.82 us -> 1.57 us
    pallas_call x1, Pallas kernels: 54.5 us -> 51.6 us  [local(): pl.pallas_call(kernel, name='layer', out_shape=(jax.ShapeDtypeStruct((16,...]
where the time goes in v2:
time: 54 us; the launch traced here: 53.8 us
  Pallas kernels  51.6 us (96%)
  local copies, waits for them, and re-layouts  1.57 us (3%)
  between operations  0.65 us (1%)
    pallas_call x1, Pallas kernels, local(): pl.pallas_call(kernel, name='layer', out_shape=(jax.ShapeDtypeStruct((16,...  51.6 us
    unnamed x2, local copies, waits for them, and re-layouts  1.57 us

profile of v2, /device:TPU:1, one launch (start us, length us, event | category | flops | bytes accessed | tf_op | source)
XLA Modules:
  0.0 53.8 jit_solution(18156903947114386676)
XLA Ops:
  0.6 51.6 %layer.1 = (bf16[16,256]{1,0:T(8,128)(2,1)S(1)}, f32[16,128,128]{2,1,0:T(8,128)S(1)}) custom-call(bf16[16,1024]{1,0:T(8,128)(2,1)} %tok_h.1, f32[16,128,128]{2,1,0:T(8,128)} %bitcast.13, bf16[1024,128]{1,0:T(8,128)(2,1)} %wq_h.1, bf16[1024,128]{1,0:T(8,128)(2,1)} %wf_h.1, bf16[1024,128]{1,0:T(8,128)(2,1)} %wi_h.1, f32[1,128]{1,0:T(1,128)} %bitcast.21, ...), custom_call_target="tpu_custom_call" | custom-call | tf_op jit(solution)/shard_map/layer/pallas_call | solution.py:435
  52.3 0.6 %copy.21 = bf16[16,256]{1,0:T(8,128)(2,1)} copy(bf16[16,256]{1,0:T(8,128)(2,1)S(1)} %get-tuple-element.10) | data formatting | bytes 16384
  52.9 1.0 %copy.22 = f32[16,1,128,128]{3,2,1,0:T(8,128)} copy(f32[16,1,128,128]{3,2,1,0:T(8,128)S(1)} %bitcast.12) | data formatting | bytes 2097152

commit v3 on v2

--- a/solution.py
+++ b/solution.py
@@ -13,7 +13,7 @@
 DIST = [0] + [(p + 1) // 2 if p % 2 else 16 - p // 2 for p in range(1, 16)]
 BACK = [DIST.index((16 - d) % 16) for d in DIST]
 FAR = list(range(15, 0, -1))
-ARRIVE = [8, 7, 6, 5, 4, 3, 2, 1, 0, 15, 14, 13, 12, 11, 10, 9]
+PASSED = [(p, p + 1) for p in (8, 7, 6, 5, 4, 3, 2, 1, 0, 15, 14, 13, 12, 11, 10, 9)]
 CHUNKS = [(4, 9), (0, 4), (13, 16), (9, 13)]
 GROUP = [4, 5, 2, 3, 6, 7, 1]
 
@@ -278,25 +278,19 @@
         due[("d2", p, j)] = both
     xb[y, 0:2, :] = d2s[0:2, :]
 
-    def forward(p):
+    def forward(p, span):
         for d in (2, 1, 3):
             post(
-                ("yf", p, d), xb.at[y, rows_of(p)], xb.at[y, rows_of(p)],
+                ("yf", p, d), xb.at[y, span], xb.at[y, span],
                 yf_s.at[p * 4 + d], yf_r.at[p * 4 + 4 - d], at_y(d),
-                xb.at[lax.rem(y + d, 4), rows_of(p)], yf_s.at[p * 4 + d], yf_r.at[p * 4 + d],
+                xb.at[lax.rem(y + d, 4), span], yf_s.at[p * 4 + d], yf_r.at[p * 4 + d],
             )
 
-    for p in ARRIVE:
-        for j in range(1, 8) if p == 0 else (0,):
-            got(("d2", p, j))
-        forward(p)
-
-    for d in (2, 1, 3):
-        post(
-            ("re", d), d1, res.at[y], re_s.at[d], re_r.at[4 - d], at_y(d),
-            res.at[lax.rem(y + d, 4)], re_s.at[d], re_r.at[d],
-        )
-    res[y] = resid
+    for lo, hi in PASSED:
+        for p in range(lo, hi):
+            for j in range(1, 8) if p == 0 else (0,):
+                got(("d2", p, j))
+        forward(lo, pl.ds(lo * 16, (hi - lo) * 16))
 
     for i in range(10, 13):
         loads[i].wait()
@@ -305,9 +299,10 @@
         loads[i].wait()
 
     def wait_rows(lo, hi):
-        for p in range(lo, hi):
-            for d in (1, 3, 2):
-                got(("yf", p, d))
+        for p, _ in PASSED:
+            if lo <= p < hi:
+                for d in (1, 3, 2):
+                    got(("yf", p, d))
 
     for n, (lo, hi) in enumerate(CHUNKS):
         wait_rows(lo, hi)
@@ -325,6 +320,13 @@
                 hb_s.at[n * 4 + d], hb_r.at[n * 4 + 4 - d], at_y(d),
                 hb.at[lax.rem(y + d, 4), span], hb_s.at[n * 4 + d], hb_r.at[n * 4 + d],
             )
+
+    for d in (2, 1, 3):
+        post(
+            ("re", d), d1, res.at[y], re_s.at[d], re_r.at[4 - d], at_y(d),
+            res.at[lax.rem(y + d, 4)], re_s.at[d], re_r.at[d],
+        )
+    res[y] = resid
 
     for n, (lo, hi) in enumerate(CHUNKS):
         span = slice(lo * 16, hi * 16)
@@ -392,6 +394,17 @@
     out_ref[...] = (d1[...].astype(F32) + mixture).astype(BF)
     for cp in sends:
         cp.wait_send()
+
+
+def store(out_ref, ns_ref, out_h, ns_h, sems):
+    copies = [pltpu.make_async_copy(out_ref, out_h, sems.at[4])]
+    for i in range(4):
+        span = pl.ds(i * 4, 4)
+        copies.append(pltpu.make_async_copy(ns_ref.at[span], ns_h.at[span], sems.at[i]))
+    for cp in copies:
+        cp.start()
+    for cp in copies:
+        cp.wait()
 
 
 def local(
@@ -462,6 +475,18 @@
         + [pltpu.SemaphoreType.REGULAR] * 2,
         compiler_params=pltpu.CompilerParams(collective_id=0, has_side_effects=True, vmem_limit_bytes=16 * 1024 * 1024),
     )(*operands)
+    layer_out, new_state = pl.pallas_call(
+        store,
+        name="store",
+        out_shape=(
+            jax.ShapeDtypeStruct((16, 256), BF),
+            jax.ShapeDtypeStruct((16, 128, 128), F32),
+        ),
+        in_specs=[pl.BlockSpec(memory_space=pltpu.VMEM)] * 2,
+        out_specs=(pl.BlockSpec(memory_space=pltpu.HBM),) * 2,
+        scratch_shapes=[dma((5,))],
+        compiler_params=pltpu.CompilerParams(vmem_limit_bytes=4 * 1024 * 1024),
+    )(layer_out, new_state)
     return layer_out, new_state.reshape(16, 1, 128, 128)
 
 

time: 54 us -> 52.9 us (0.980)
  local copies, waits for them, and re-layouts: 1.57 us -> 0 us
  Pallas kernels: 51.6 us -> 52.2 us
    unnamed x2 -> x0, local copies, waits for them, and re-layouts: 1.57 us -> none
    pallas_call x0 -> x1, Pallas kernels: none -> 1.01 us  [local(): pl.pallas_call(store, name='store', out_shape=(jax.ShapeDtypeStruct((16,...]
where the time goes in v3:
time: 52.9 us; the launch traced here: 52.8 us
  Pallas kernels  52.2 us (99%)
  between operations  0.64 us (1%)
    pallas_call x1, Pallas kernels, local(): pl.pallas_call(kernel, name='layer', out_shape=(jax.ShapeDtypeStruct((16,...  51.2 us

profile of v3, /device:TPU:1, one launch (start us, length us, event | category | flops | bytes accessed | tf_op | source)
XLA Modules:
  0.0 52.8 jit_solution(5182326775723619392)
XLA Ops:
  0.6 51.2 %layer.1 = (bf16[16,256]{1,0:T(8,128)(2,1)S(1)}, f32[16,128,128]{2,1,0:T(8,128)S(1)}) custom-call(bf16[16,1024]{1,0:T(8,128)(2,1)} %tok_h.1, f32[16,128,128]{2,1,0:T(8,128)} %bitcast.12, bf16[1024,128]{1,0:T(8,128)(2,1)} %wq_h.1, bf16[1024,128]{1,0:T(8,128)(2,1)} %wf_h.1, bf16[1024,128]{1,0:T(8,128)(2,1)} %wi_h.1, f32[1,128]{1,0:T(1,128)} %bitcast.20, ...), custom_call_target="tpu_custom_call" | custom-call | tf_op jit(solution)/shard_map/layer/pallas_call | solution.py:448
  51.8 1.0 %store.1 = (bf16[16,256]{1,0:T(8,128)(2,1)}, f32[16,128,128]{2,1,0:T(8,128)}) custom-call(bf16[16,256]{1,0:T(8,128)(2,1)S(1)} %get-tuple-element.6.out_ref, f32[16,128,128]{2,1,0:T(8,128)S(1)} %get-tuple-element.7.ns_ref), custom_call_target="tpu_custom_call" | custom-call | tf_op jit(solution)/shard_map/store/pallas_call | solution.py:478
